TPU v7x, 32 devices: a whole 2x2x4 slice. The times are simulated.
32 devices in a mesh: sp: 16 (over z, y, x), tp: 2 (over core).
Axes of the slice: x: 2, y: 2, z: 4, core: 2. Of those that a mesh axis runs over, the one named last changes fastest.
Arguments:
- mixer_in: bfloat16 [8192, 1024], P('sp', 'tp'), may hold values from -6 to 6
- residual: bfloat16 [8192, 2048], P(('sp', 'tp')), may hold values from -6 to 6
- decay_real: float32 [64, 64], P('tp'), may hold values from -2 to 0, as said below
- decay_imag: float32 [64, 64], P('tp'), may hold values from 1 to 200
- log_step: float32 [64], P('tp'), may hold values from -3.9 to -2.5
- in_real: float32 [64, 64, 16], P('tp'), may hold values from -1 to 1
- in_imag: float32 [64, 64, 16], P('tp'), may hold values from -1 to 1
- output_real: float32 [64, 16, 64], P('tp'), may hold values from -0.5 to 0.5
- output_imaginary: float32 [64, 16, 64], P('tp'), may hold values from -0.5 to 0.5
- skip: float32 [1024], P('tp'), may hold values from -4 to 4
- out_proj: bfloat16 [1024, 2048], P('tp'), may hold values from -0.1875 to 0.1875
- norm_gain: float32 [2048], replicated, may hold values from 0.1 to 1.9
- w_gate: bfloat16 [2048, 5632], P('sp', 'tp'), may hold values from -0.125 to 0.125
- w_up: bfloat16 [2048, 5632], P('sp', 'tp'), may hold values from -0.125 to 0.125
- w_down: bfloat16 [5632, 2048], P('tp', 'sp'), may hold values from -0.078125 to 0.078125
Outputs:
- output: bfloat16 [8192, 2048], P(('sp', 'tp'))
Inputs may be any that keep to these rules, and one draw needn't show every extreme that they name: `decay_real`: every entry is negative.
All inputs are finite; a program needn't handle non-finite values.
Results may differ from a plain program's by a relative error of at most 0.02.
Values may be sent and summed in bfloat16 or wider, within the bound.
A program may use at most 128 MiB of HBM per device.

v0:
```python
import jax
import jax.numpy as jnp
from jax import lax
from jax.sharding import PartitionSpec as P


def prefix(value, axis, join, neutral):
    count, mine = (lax.axis_size(axis), lax.axis_index(axis))
    pieces = jax.tree.map(lambda part: lax.all_gather(part, axis), value)
    subtotal = jax.tree.map(
        lambda part, zero: jnp.full_like(part, 0) + jnp.asarray(zero, part.dtype), value, neutral
    )

    def step(position, subtotal):
        longer = join(subtotal, jax.tree.map(lambda part: part[position], pieces))
        return jax.tree.map(lambda new, old: jnp.where(position < mine, new, old), longer, subtotal)

    return lax.fori_loop(0, count - 1, step, subtotal)


def discrete(decay_real, decay_imag, log_step, in_real, in_imag):
    step_size = jnp.exp(log_step)[:, None]
    magnitude = jnp.exp(decay_real * step_size)
    angle = decay_imag * step_size
    power_re = magnitude * jnp.cos(angle)
    power_im = magnitude * jnp.sin(angle)
    denom = decay_real * decay_real + decay_imag * decay_imag
    ratio_re = ((power_re - 1.0) * decay_real + power_im * decay_imag) / denom
    ratio_im = (power_im * decay_real - (power_re - 1.0) * decay_imag) / denom
    drive_re = ratio_re[..., None] * in_real - ratio_im[..., None] * in_imag
    drive_im = ratio_re[..., None] * in_imag + ratio_im[..., None] * in_real
    return (power_re, power_im, drive_re, drive_im)


def combine(earlier, later):
    ar1, ai1, br1, bi1 = earlier
    ar2, ai2, br2, bi2 = later
    return (
        ar2 * ar1 - ai2 * ai1,
        ar2 * ai1 + ai2 * ar1,
        ar2 * br1 - ai2 * bi1 + br2,
        ar2 * bi1 + ai2 * br1 + bi2,
    )


def spread_blocks(matrix):
    groups = matrix.shape[0]
    unit_blocks = jnp.eye(groups, dtype=jnp.float32)[:, None, :, None]
    turned = jnp.transpose(matrix, (0, 2, 1))[:, :, None, :]
    return (unit_blocks * turned).reshape(groups * matrix.shape[2], groups * matrix.shape[1])


def local_states(power_re, power_im, drive_re, drive_im):
    rows, flat_size = drive_re.shape
    span = 8
    blocks = rows // span
    dr = drive_re.reshape(blocks, span, flat_size)
    di = drive_im.reshape(blocks, span, flat_size)
    cur_re = dr[:, 0]
    cur_im = di[:, 0]
    inner_re = [cur_re]
    inner_im = [cur_im]
    lift_re = [power_re]
    lift_im = [power_im]
    for index in range(1, span):
        cur_re, cur_im = (
            power_re * cur_re - power_im * cur_im + dr[:, index],
            power_re * cur_im + power_im * cur_re + di[:, index],
        )
        inner_re.append(cur_re)
        inner_im.append(cur_im)
        prev_re, prev_im = (lift_re[-1], lift_im[-1])
        lift_re.append(power_re * prev_re - power_im * prev_im)
        lift_im.append(power_re * prev_im + power_im * prev_re)
    inner_re = jnp.stack(inner_re, axis=1)
    inner_im = jnp.stack(inner_im, axis=1)
    lift_re = jnp.concatenate(lift_re, axis=0)[None]
    lift_im = jnp.concatenate(lift_im, axis=0)[None]
    block_re = jnp.broadcast_to(lift_re[0, span - 1][None], (blocks, flat_size))
    block_im = jnp.broadcast_to(lift_im[0, span - 1][None], (blocks, flat_size))
    totals = (block_re, block_im, cur_re, cur_im)
    distance = 1
    while distance < blocks:
        ones = jnp.ones((distance, flat_size), jnp.float32)
        zeros = jnp.zeros((distance, flat_size), jnp.float32)
        moved = (
            jnp.concatenate([ones, totals[0][:-distance]], axis=0),
            jnp.concatenate([zeros, totals[1][:-distance]], axis=0),
            jnp.concatenate([zeros, totals[2][:-distance]], axis=0),
            jnp.concatenate([zeros, totals[3][:-distance]], axis=0),
        )
        totals = combine(moved, totals)
        distance = distance * 2
    one_row = jnp.ones((1, flat_size), jnp.float32)
    zero_row = jnp.zeros((1, flat_size), jnp.float32)
    before_a_re = jnp.concatenate([one_row, totals[0][:-1]], axis=0)[:, None]
    before_a_im = jnp.concatenate([zero_row, totals[1][:-1]], axis=0)[:, None]
    before_re = jnp.concatenate([zero_row, totals[2][:-1]], axis=0)[:, None]
    before_im = jnp.concatenate([zero_row, totals[3][:-1]], axis=0)[:, None]
    state_real = inner_re + lift_re * before_re - lift_im * before_im
    state_imaginary = inner_im + lift_re * before_im + lift_im * before_re
    pw_re = lift_re * before_a_re - lift_im * before_a_im
    pw_im = lift_re * before_a_im + lift_im * before_a_re
    summary = (totals[0][-1], totals[1][-1], totals[2][-1], totals[3][-1])
    return (
        pw_re.reshape(rows, flat_size),
        pw_im.reshape(rows, flat_size),
        state_real.reshape(rows, flat_size),
        state_imaginary.reshape(rows, flat_size),
        summary,
    )


def on_device(
    mixer_in,
    residual,
    decay_real,
    decay_imag,
    log_step,
    in_real,
    in_imag,
    output_real,
    output_imaginary,
    skip,
    out_proj,
    norm_gain,
    w_gate,
    w_up,
    w_down,
):
    highest_precision = lax.Precision.HIGHEST
    power_re, power_im, bar_re, bar_im = discrete(
        decay_real, decay_imag, log_step, in_real, in_imag
    )
    flat_size = decay_real.shape[0] * decay_real.shape[1]
    read_in = jnp.concatenate([spread_blocks(bar_re), spread_blocks(bar_im)], axis=1)
    signal = mixer_in.astype(jnp.float32)
    drive = jnp.dot(signal, read_in, precision=highest_precision)
    drive_re = drive[:, :flat_size]
    drive_im = drive[:, flat_size:]
    pw_re, pw_im, state_real, state_imaginary, summary = local_states(
        power_re.reshape(1, flat_size), power_im.reshape(1, flat_size), drive_re, drive_im
    )
    zero_line = jnp.zeros((flat_size,), jnp.float32)
    identity = (jnp.ones((flat_size,), jnp.float32), zero_line, zero_line, zero_line)
    _, _, hold_re, hold_im = prefix(summary, "sp", combine, identity)
    state_real = state_real + pw_re * hold_re[None] - pw_im * hold_im[None]
    state_imaginary = state_imaginary + pw_re * hold_im[None] + pw_im * hold_re[None]
    read_out = jnp.concatenate(
        [spread_blocks(output_real), -spread_blocks(output_imaginary)], axis=0
    )
    mixed_before_norm = jnp.dot(
        jnp.concatenate([state_real, state_imaginary], axis=1),
        read_out,
        precision=highest_precision,
    )
    mixed_before_norm = mixed_before_norm + skip[None] * signal
    activated = jax.nn.gelu(mixed_before_norm).astype(jnp.bfloat16)
    partial_value = jnp.dot(activated, out_proj, preferred_element_type=jnp.float32).astype(
        jnp.bfloat16
    )
    mixed = lax.psum_scatter(
        lax.optimization_barrier(partial_value).astype(jnp.float32).astype(jnp.bfloat16),
        "tp",
        scatter_dimension=0,
        tiled=True,
    )
    carried = residual.astype(jnp.float32) + mixed.astype(jnp.float32)
    scale = lax.rsqrt(jnp.mean(carried * carried, axis=-1, keepdims=True) + 1e-06)
    normed = (carried * scale * norm_gain).astype(jnp.bfloat16)
    full_rows = lax.all_gather(normed, "tp", axis=0, tiled=True)
    gate = jnp.dot(
        full_rows,
        lax.all_gather(w_gate, "sp", axis=0, tiled=True),
        preferred_element_type=jnp.float32,
    )
    up = jnp.dot(
        full_rows,
        lax.all_gather(w_up, "sp", axis=0, tiled=True),
        preferred_element_type=jnp.float32,
    )
    down_columns = lax.all_gather(w_down, "sp", axis=1, tiled=True)
    hidden = (jax.nn.silu(gate) * up).astype(jnp.bfloat16)
    partial_value = jnp.dot(hidden, down_columns, preferred_element_type=jnp.float32).astype(
        jnp.bfloat16
    )
    down = lax.psum_scatter(
        lax.optimization_barrier(partial_value).astype(jnp.float32).astype(jnp.bfloat16),
        "tp",
        scatter_dimension=0,
        tiled=True,
    )
    return (carried + 0.5 * down.astype(jnp.float32)).astype(jnp.bfloat16)


def solution(mesh):
    return jax.shard_map(
        on_device,
        mesh=mesh,
        in_specs=(
            P("sp", "tp"),
            P(("sp", "tp"), None),
            P("tp", None),
            P("tp", None),
            P("tp"),
            P("tp", None, None),
            P("tp", None, None),
            P("tp", None, None),
            P("tp", None, None),
            P("tp"),
            P("tp", None),
            P(),
            P("sp", "tp"),
            P("sp", "tp"),
            P("tp", "sp"),
        ),
        out_specs=P(("sp", "tp"), None),
        check_vma=False,
    )
```

profile of v0, /device:TPU:0, one launch (start us, length us, event | category | flops | bytes accessed | tf_op | source)
XLA Modules:
  0.0 897.7 jit_solution(369592521946466958)
XLA Ops:
  7.4 0.9 cosine_multiply_fusion
  8.6 1.1 subtract_bitcast_fusion
  9.7 8.3 broadcast_multiply_fusion.2
  18.1 7.8 mul.1865
  25.9 7.9 mul.1870
  33.8 10.5 %fusion.11 = f32[512,4096]{1,0:T(8,128)S(1)} fusion(bf16[512,512]{1,0:T(8,128)(2,1)S(1)} %copy-done.39, f32[512,2048]{1,0:T(8,128)} %mul.1870, f32[512,2048]{1,0:T(8,128)} %mul.1865), kind=kOutput, calls=%fused_computation.18 | convolution fusion | flops 12886999040 | bytes 17301504 | tf_op jit(solution)/shard_map/dot_general | solution.py:138
  44.2 1.1 slice_bitcast_fusion.1
  45.4 2.5 fusion.61
  47.9 2.7 fusion.62
  50.6 3.0 bitcast_add_fusion.9
  53.6 5.1 multiply_subtract_fusion.3
  58.8 1.4 copy.111
  61.5 6.1 copy_add_fusion.1
  67.6 1.8 bitcast_add_fusion.1
  72.5 1.0 fusion.40
  74.3 0.9 fusion.38
  76.0 2.5 copy.103
  78.5 2.4 copy.106
  80.9 2.4 copy.107
  83.3 2.4 copy.108
  85.8 1.4 copy.109
  87.1 1.3 copy.110
  89.2 43.1 %all-gather.2 = f32[16,1,2048]{2,1,0:T(1,128)S(1)} all-gather(f32[1,1,2048]{2,1,0:T(1,128)S(1)} %slice_bitcast_fusion.3), channel_id=1, replica_groups=mesh['sp'=16,'tp'=2] {'sp'}, dimensions={0}, use_global_device_ids=true | all-gather | bytes 139264 | tf_op jit(solution)/shard_map/all_gather | solution.py:9
  132.3 36.1 %all-gather.1 = f32[16,1,2048]{2,1,0:T(1,128)S(1)} all-gather(f32[1,1,2048]{2,1,0:T(1,128)S(1)} %slice_bitcast_fusion.4), channel_id=1, replica_groups=mesh['sp'=16,'tp'=2] {'sp'}, dimensions={0}, use_global_device_ids=true | all-gather | bytes 139264 | tf_op jit(solution)/shard_map/all_gather | solution.py:9
  168.5 38.2 %all-gather = f32[16,1,2048]{2,1,0:T(1,128)S(1)} all-gather(f32[1,1,2048]{2,1,0:T(1,128)S(1)} %slice_bitcast_fusion.5), channel_id=1, replica_groups=mesh['sp'=16,'tp'=2] {'sp'}, dimensions={0}, use_global_device_ids=true | all-gather | bytes 139264 | tf_op jit(solution)/shard_map/all_gather | solution.py:9
  207.5 36.2 %all-gather.3 = f32[16,1,2048]{2,1,0:T(1,128)S(1)} all-gather(f32[1,1,2048]{2,1,0:T(1,128)S(1)} %slice_bitcast_fusion.2), channel_id=1, replica_groups=mesh['sp'=16,'tp'=2] {'sp'}, dimensions={0}, use_global_device_ids=true | all-gather | bytes 139264 | tf_op jit(solution)/shard_map/all_gather | solution.py:9
  244.3 26.6 %while.16 = (s32[]{:T(128)}, f32[2048]{0:T(1024)S(1)}, f32[2048]{0:T(1024)S(1)}, s32[]{:T(128)}, f32[16,2048]{1,0:T(8,128)}, /*index=5*/f32[16,2048]{1,0:T(8,128...) while((s32[]{:T(128)}, f32[2048]{0:T(1024)S(1)}, f32[2048]{0:T(1024)S(1)}, ...), condition=%wide.region_1.2_spmd.clone, body=%wide.region_0.1_spmd.clone.sunk | while | flops 24580 | bytes 131201 | solution.py:18
  245.4 0.9 constant_dynamic-slice_fusion.7
  247.1 0.9 constant_dynamic-slice_fusion.7
  248.9 0.9 constant_dynamic-slice_fusion.7
  250.7 0.9 constant_dynamic-slice_fusion.7
  254.2 0.9 constant_dynamic-slice_fusion.7
  256.0 0.9 constant_dynamic-slice_fusion.7
  266.5 0.9 constant_dynamic-slice_fusion.7
  268.3 0.9 constant_dynamic-slice_fusion.7
  271.0 2.0 concatenate.124
  273.0 1.9 concatenate.129
  275.0 1.9 concatenate.125
  276.8 2.4 copy.100
  279.2 1.4 copy.101
  280.6 1.3 copy.102
  282.0 1.3 copy.98
  283.3 1.3 copy.99
  284.8 8.1 broadcast_multiply_fusion
  293.0 7.8 mul.2031
  300.8 7.8 neg.11
  308.6 1.9 concatenate.128
  310.5 11.9 %stack.5 = f32[64,8,2048]{2,1,0:T(8,128)} concatenate(f32[64,1,2048]{2,1,0:T(1,128)S(1)} %get-tuple-element.246, f32[64,1,2048]{2,1,0:T(1,128)} %copy.106, f32[64,1,2048]{2,1,0:T(1,128)} %copy.107, f32[64,1,2048]{2,1,0:T(1,128)} %copy.108, f32[64,1,2048]{2,1,0:T(1,128)} %copy.109, f32[64,1,2048]{2,1,0:T(1,128)} %copy.110, f32[64,1,2048]{2,1,0:T(1,128)} %copy.111, ...), dimensions={1} | concatenate | bytes 8388608 | tf_op jit(solution)/shard_map/stack | solution.py:76
  322.4 12.0 %stack.4 = f32[64,8,2048]{2,1,0:T(8,128)} concatenate(f32[64,1,2048]{2,1,0:T(1,128)S(1)} %get-tuple-element.248, f32[64,1,2048]{2,1,0:T(1,128)} %copy.98, f32[64,1,2048]{2,1,0:T(1,128)} %copy.99, f32[64,1,2048]{2,1,0:T(1,128)} %copy.100, f32[64,1,2048]{2,1,0:T(1,128)} %copy.101, f32[64,1,2048]{2,1,0:T(1,128)} %copy.102, f32[64,1,2048]{2,1,0:T(1,128)} %copy.103, ...), dimensions={1} | concatenate | bytes 8388608 | tf_op jit(solution)/shard_map/stack | solution.py:75
  334.4 7.0 fusion.15
  341.4 0.9 copy-done.22
  342.3 16.5 %fusion.24 = bf16[512,512]{1,0:T(8,128)(2,1)S(1)} fusion(bf16[512,512]{1,0:T(8,128)(2,1)S(1)} %copy-done.40, f32[2048,512]{0,1:T(8,128)S(1)} %copy-done.22, f32[2048,512]{0,1:T(8,128)S(1)} %copy-done.21, f32[512,2048]{1,0:T(8,128)} %get-tuple-element.258, f32[512,2048]{1,0:T(8,128)S(1)} %get-tuple-element.257, f32[512]{0:T(512)S(1)} %copy-done.50), kind=kOutput, calls=%fused_computation.49 | convolution fusion | flops 12892241920 | bytes 17827840 | tf_op jit(solution)/shard_map/dot_general | solution.py:152
  358.8 2.6 convolution_convert_fusion.1
  361.5 7.6 reduce-scatter.3.cloned.1.call-done
  369.1 1.6 multiply_reduce_fusion
  370.8 2.6 multiply_convert_fusion.1
  375.3 10.1 %all-gather.9.cloned.1.call-done = bf16[512,2048]{1,0:T(8,128)(2,1)} async-done(((bf16[256,2048]{1,0:T(8,128)(2,1)}), bf16[512,2048]{1,0:T(8,128)(2,1)}) %all-gather.9.cloned.1.call-update) | async-done | bytes 2097168 | tf_op jit(solution)/shard_map/all_gather | solution.py:171
  385.4 145.4 %all-gather.11.cloned.1.call-done = bf16[2048,2816]{1,0:T(8,128)(2,1)} async-done(((bf16[128,2816]{1,0:T(8,128)(2,1)}), bf16[2048,2816]{1,0:T(8,128)(2,1)}) %all-gather.11.cloned.1.call-update) | async-done | bytes 11534352 | tf_op jit(solution)/shard_map/all_gather | solution.py:174
  530.8 12.7 %fusion.63 = f32[512,2816]{1,0:T(8,128)} fusion(bf16[512,2048]{1,0:T(8,128)(2,1)} %all-gather.9.cloned.1.call-done, bf16[2048,2816]{1,0:T(8,128)(2,1)} %all-gather.11.cloned.1.call-done), kind=kOutput, calls=%fused_computation.183 | convolution fusion | flops 5905580032 | bytes 19398656 | tf_op jit(solution)/shard_map/dot_general | solution.py:172
  543.5 129.6 %all-gather.13.cloned.1.call-done = bf16[2048,2816]{1,0:T(8,128)(2,1)} async-done(((bf16[128,2816]{1,0:T(8,128)(2,1)}), bf16[2048,2816]{1,0:T(8,128)(2,1)}) %all-gather.13.cloned.1.call-update) | async-done | bytes 11534352 | tf_op jit(solution)/shard_map/all_gather | solution.py:179
  673.0 182.8 %all-gather.15.cloned.1.call-done = bf16[2816,2048]{1,0:T(8,128)(2,1)} async-done(((bf16[2816,128]{1,0:T(8,128)(2,1)}), bf16[2816,2048]{1,0:T(8,128)(2,1)}) %all-gather.15.cloned.1.call-update) | async-done | bytes 11534352 | tf_op jit(solution)/shard_map/all_gather | solution.py:182
  855.8 23.4 %convolution_convert_fusion = bf16[512,2048]{1,0:T(8,128)(2,1)} fusion(bf16[2816,2048]{1,0:T(8,128)(2,1)} %all-gather.15.cloned.1.call-done, f32[512,2816]{1,0:T(8,128)} %fusion.63, bf16[512,2048]{1,0:T(8,128)(2,1)} %all-gather.9.cloned.1.call-done, bf16[2048,2816]{1,0:T(8,128)(2,1)} %all-gather.13.cloned.1.call-done), kind=kOutput, calls=%fused_computation.35 | convolution fusion | flops 11820859392 | bytes 33030144 | tf_op jit(solution)/shard_map/dot_general | solution.py:184
  879.2 8.1 reduce-scatter.5.cloned.1.call-done
  887.3 3.1 add_convert_fusion
  (200 shorter events, 30.4 us)
Async XLA Ops:
  6.5 352.3 %copy-start = (bf16[512,2048]{1,0:T(8,128)(2,1)S(1)}, bf16[512,2048]{1,0:T(8,128)(2,1)}, u32[]{:S(2)}) copy-start(bf16[512,2048]{1,0:T(8,128)(2,1)} %param.27) | copy-start | bytes 6291460
  6.5 362.6 %reduce-scatter.3.cloned.1.call-start = ((), (), s32[]{:S(2)}) async-start(), calls=%async_computation.2 | async-start | bytes 3145728 | tf_op jit(solution)/shard_map/reduce_scatter | solution.py:162
  6.5 11.5 %copy-start.47 = (f32[32,32]{0,1:T(8,128)}, f32[32,32]{0,1:T(8,128)S(1)}, u32[]{:S(2)}) copy-start(f32[32,32]{0,1:T(8,128)S(1)} %fusion.52) | copy-start | bytes 12292
  25.9 7.9 copy-start.39
  45.3 5.2 copy-start.1
  45.3 5.2 copy-start.2
  47.8 5.8 copy-start.4
  47.8 5.8 copy-start.12
  47.9 5.8 copy-start.14
  50.6 8.2 copy-start.6
  50.6 8.2 copy-start.16
  50.6 8.2 copy-start.18
  58.8 1.4 copy-start.20
  61.2 8.2 copy-start.41
  61.4 8.1 copy-start.43
  61.4 6.2 copy-start.5
  61.4 6.2 copy-start.7
  61.4 6.2 copy-start.13
  61.4 6.2 copy-start.15
  61.4 6.2 copy-start.17
  61.4 6.2 copy-start.19
  61.5 6.2 copy-start.29
  61.5 6.2 copy-start.30
  73.5 0.8 copy-start.10
  73.5 1.7 copy-start.8
  76.0 9.8 %copy-start.36 = (f32[64,1,2048]{2,0,1:T(8,128)S(1)}, f32[64,1,2048]{2,0,1:T(8,128)}, u32[]{:S(2)}) copy-start(f32[64,1,2048]{2,0,1:T(8,128)} %get-tuple-element.196) | copy-start | bytes 1572868
  76.0 11.2 %copy-start.35 = (f32[64,1,2048]{2,0,1:T(8,128)S(1)}, f32[64,1,2048]{2,0,1:T(8,128)}, u32[]{:S(2)}) copy-start(f32[64,1,2048]{2,0,1:T(8,128)} %get-tuple-element.194) | copy-start | bytes 1572868
  76.0 12.5 %copy-start.24 = (f32[64,2048]{1,0:T(8,128)S(1)}, f32[64,2048]{1,0:T(8,128)}, u32[]{:S(2)}) copy-start(f32[64,2048]{1,0:T(8,128)} %fusion.38) | copy-start | bytes 1572868
  76.0 12.5 %copy-start.23 = (f32[64,2048]{1,0:T(8,128)S(1)}, f32[64,2048]{1,0:T(8,128)}, u32[]{:S(2)}) copy-start(f32[64,2048]{1,0:T(8,128)} %get-tuple-element.206) | copy-start | bytes 1572868
  76.0 12.5 %copy-start.9 = (f32[64,2048]{1,0:T(8,128)S(1)}, f32[64,2048]{1,0:T(8,128)}, u32[]{:S(2)}) copy-start(f32[64,2048]{1,0:T(8,128)} %copy-done.8) | copy-start | bytes 1572868
  76.0 12.5 %copy-start.11 = (f32[64,2048]{1,0:T(8,128)S(1)}, f32[64,2048]{1,0:T(8,128)}, u32[]{:S(2)}) copy-start(f32[64,2048]{1,0:T(8,128)} %copy-done.10) | copy-start | bytes 1572868
  76.0 12.5 %copy-start.38 = (f32[48,2048]{1,0:T(8,128)S(1)}, f32[48,2048]{1,0:T(8,128)}, u32[]{:S(2)}) copy-start(f32[48,2048]{1,0:T(8,128)} %slice.234) | copy-start | bytes 1179652
  88.8 118.6 %copy-start.25 = (f32[64,2048]{1,0:T(8,128)}, f32[64,2048]{1,0:T(8,128)S(1)}, u32[]{:S(2)}) copy-start(f32[64,2048]{1,0:T(8,128)S(1)} %get-tuple-element.203) | copy-start | bytes 1572868
  89.1 118.3 %copy-start.26 = (f32[64,2048]{1,0:T(8,128)}, f32[64,2048]{1,0:T(8,128)S(1)}, u32[]{:S(2)}) copy-start(f32[64,2048]{1,0:T(8,128)S(1)} %get-tuple-element.262) | copy-start | bytes 1572868
  89.1 154.5 %copy-start.27 = (f32[64,2048]{1,0:T(8,128)}, f32[64,2048]{1,0:T(8,128)S(1)}, u32[]{:S(2)}) copy-start(f32[64,2048]{1,0:T(8,128)S(1)} %get-tuple-element.261) | copy-start | bytes 1572868
  89.1 154.5 %copy-start.28 = (f32[64,2048]{1,0:T(8,128)}, f32[64,2048]{1,0:T(8,128)S(1)}, u32[]{:S(2)}) copy-start(f32[64,2048]{1,0:T(8,128)S(1)} %get-tuple-element.267) | copy-start | bytes 1572868
  271.0 8.2 copy-start.34
  271.0 9.6 %copy-start.33 = (f32[64,1,2048]{2,0,1:T(8,128)S(1)}, f32[64,1,2048]{2,0,1:T(8,128)}, u32[]{:S(2)}) copy-start(f32[64,1,2048]{2,0,1:T(8,128)} %get-tuple-element.193) | copy-start | bytes 1572868
  271.0 11.0 %copy-start.32 = (f32[64,1,2048]{2,0,1:T(8,128)S(1)}, f32[64,1,2048]{2,0,1:T(8,128)}, u32[]{:S(2)}) copy-start(f32[64,1,2048]{2,0,1:T(8,128)} %get-tuple-element.201) | copy-start | bytes 1572868
  271.0 12.3 %copy-start.31 = (f32[64,1,2048]{2,0,1:T(8,128)S(1)}, f32[64,1,2048]{2,0,1:T(8,128)}, u32[]{:S(2)}) copy-start(f32[64,1,2048]{2,0,1:T(8,128)} %get-tuple-element.199) | copy-start | bytes 1572868
  271.0 13.6 %copy-start.45 = (f32[32,16,64]{2,1,0:T(8,128)S(1)}, f32[32,16,64]{2,1,0:T(8,128)}, u32[]{:S(2)}) copy-start(f32[32,16,64]{2,1,0:T(8,128)} %param.24) | copy-start | bytes 393220
  273.0 11.7 %copy-start.46 = (f32[32,16,64]{2,1,0:T(8,128)S(1)}, f32[32,16,64]{2,1,0:T(8,128)}, u32[]{:S(2)}) copy-start(f32[32,16,64]{2,1,0:T(8,128)} %param.25) | copy-start | bytes 393220
  273.0 11.8 %copy-start.48 = (f32[32,32]{0,1:T(8,128)S(1)}, f32[32,32]{0,1:T(8,128)}, u32[]{:S(2)}) copy-start(f32[32,32]{0,1:T(8,128)} %copy-done.47) | copy-start | bytes 12292
  322.4 12.0 %copy-start.37 = (f32[64,2048]{1,0:T(8,128)S(1)}, f32[64,2048]{1,0:T(8,128)}, u32[]{:S(2)}) copy-start(f32[64,2048]{1,0:T(8,128)} %concatenate.124) | copy-start | bytes 1572868
  322.4 12.0 %copy-start.42 = (f32[8,2048]{1,0:T(8,128)S(1)}, f32[8,2048]{1,0:T(8,128)}, u32[]{:S(2)}) copy-start(f32[8,2048]{1,0:T(8,128)} %copy-done.41) | copy-start | bytes 196612
  322.4 12.0 %copy-start.44 = (f32[8,2048]{1,0:T(8,128)S(1)}, f32[8,2048]{1,0:T(8,128)}, u32[]{:S(2)}) copy-start(f32[8,2048]{1,0:T(8,128)} %copy-done.43) | copy-start | bytes 196612
  334.3 7.0 copy-start.21
  334.4 7.9 copy-start.22
  334.4 7.9 copy-start.40
  334.4 7.9 copy-start.50
  358.8 10.3 %copy-start.3 = (bf16[256,2048]{1,0:T(8,128)(2,1)S(1)}, bf16[256,2048]{1,0:T(8,128)(2,1)}, u32[]{:S(2)}) copy-start(bf16[256,2048]{1,0:T(8,128)(2,1)} %param.18) | copy-start | bytes 3145732
  361.4 9.3 %copy-start.49 = (f32[2048]{0:T(1024)S(1)}, f32[2048]{0:T(1024)}, u32[]{:S(2)}) copy-start(f32[2048]{0:T(1024)} %param.28) | copy-start | bytes 24580
  361.4 23.9 %all-gather.9.cloned.1.call-start = ((), (), s32[]{:S(2)}) async-start(), calls=%async_computation.3 | async-start | bytes 3145728 | tf_op jit(solution)/shard_map/all_gather | solution.py:171
  373.4 157.4 %all-gather.11.cloned.1.call-start = ((), (), s32[]{:S(2)}) async-start(), calls=%async_computation.4 | async-start | bytes 12255232 | tf_op jit(solution)/shard_map/all_gather | solution.py:174
  374.1 298.9 %all-gather.13.cloned.1.call-start = ((), (), s32[]{:S(2)}) async-start(), calls=%async_computation.5 | async-start | bytes 12255232 | tf_op jit(solution)/shard_map/all_gather | solution.py:179
  374.7 481.1 %all-gather.15.cloned.1.call-start = ((), (), s32[]{:S(2)}) async-start(), calls=%async_computation.6 | async-start | bytes 12255232 | tf_op jit(solution)/shard_map/all_gather | solution.py:182
  375.3 512.1 %reduce-scatter.5.cloned.1.call-start = ((), (), s32[]{:S(2)}) async-start(), calls=%async_computation.7 | async-start | bytes 3145728 | tf_op jit(solution)/shard_map/reduce_scatter | solution.py:187
Sparse Core Ops, SparseCore 0:
  361.6 7.4 reduce-scatter.2
  373.5 11.8 all-gather.8
  388.1 142.5 all-gather.10
  533.4 139.5 all-gather.12
  675.6 180.2 all-gather.14
  879.3 7.9 reduce-scatter.4
where the time goes:
time: 910 us; the launch traced here: 898 us
  waiting for transfers between devices  485 us (53%)
  blocking collectives  154 us (17%)
  local copies, waits for them, and re-layouts  123 us (14%)
  matrix products  65.6 us (7%)
  other arithmetic  54.9 us (6%)
  between operations  14.7 us (2%)
    all_gather x1, waiting for transfers between devices, on_device(): down_columns = lax.all_gather(w_down, 'sp', axis=1, tiled=True)  183 us
    all_gather x4, blocking collectives, prefix(): pieces = jax.tree.map(lambda part: lax.all_gather(part, axis), value)  154 us
    all_gather x1, waiting for transfers between devices, on_device(): lax.all_gather(w_gate, 'sp', axis=0, tiled=True)  145 us
    all_gather x1, waiting for transfers between devices, on_device(): lax.all_gather(w_up, 'sp', axis=0, tiled=True)  130 us
    dynamic_slice x30, local copies, waits for them, and re-layouts, step(): longer = join(subtotal, jax.tree.map(lambda part: part[position], pieces))  25.8 us
    mul x3, local copies, waits for them, and re-layouts, spread_blocks(): unit_blocks * turned  23.5 us
    dot_general x1, matrix products, on_device(): jnp.dot(hidden, down_columns, preferred_element_type=jnp.float32)  23.4 us
  transfers between devices with their start and end apart: 6, of which 6 were waited for; matrix products, arithmetic and copies ran while one was open for 1% of the time, Pallas kernels for 0%

commit v1 on v0

--- a/solution.py
+++ b/solution.py
@@ -2,6 +2,23 @@
 import jax.numpy as jnp
 from jax import lax
 from jax.sharding import PartitionSpec as P
+
+
+def laid_out(blocks, dim):
+    dims = list(blocks.shape[1:])
+    dims[dim] *= blocks.shape[0]
+    return jnp.moveaxis(blocks, 0, dim).reshape(dims)
+
+
+def gather_around(x, axis, dim):
+    length = lax.axis_size(axis)
+    right = [(i, (i + 1) % length) for i in range(length)]
+    pieces = [x]
+    while len(pieces) < length:
+        pieces.append(lax.ppermute(pieces[-1], axis, right))
+    index = lax.axis_index(axis)
+    pieces = jnp.stack(pieces)[(index - jnp.arange(length)) % length]
+    return laid_out(pieces, dim)
 
 
 def prefix(value, axis, join, neutral):
@@ -179,7 +196,7 @@
         lax.all_gather(w_up, "sp", axis=0, tiled=True),
         preferred_element_type=jnp.float32,
     )
-    down_columns = lax.all_gather(w_down, "sp", axis=1, tiled=True)
+    down_columns = gather_around(w_down, "sp", 1)
     hidden = (jax.nn.silu(gate) * up).astype(jnp.bfloat16)
     partial_value = jnp.dot(hidden, down_columns, preferred_element_type=jnp.float32).astype(
         jnp.bfloat16

time: 910 us -> 959 us (1.054)
  local copies, waits for them, and re-layouts: 123 us -> 168 us
    ppermute x0 -> x15, waiting for transfers between devices: none -> 463 us  [gather_around(): pieces.append(lax.ppermute(pieces[-1], axis, right))]
    all_gather x1 -> x0, waiting for transfers between devices: 183 us -> none  [on_device(): down_columns = lax.all_gather(w_down, 'sp', axis=1, tiled=True)]
    all_gather x1, waiting for transfers between devices: 145 us -> 0.01 us  [on_device(): lax.all_gather(w_gate, 'sp', axis=0, tiled=True)]
    all_gather x1, waiting for transfers between devices: 130 us -> 0.01 us  [on_device(): lax.all_gather(w_up, 'sp', axis=0, tiled=True)]
    transpose x0 -> x1, local copies, waits for them, and re-layouts: none -> 14.9 us  [laid_out(): return jnp.moveaxis(blocks, 0, dim).reshape(dims)]
    unnamed x110 -> x109, local copies, waits for them, and re-layouts: 3.38 us -> 17.7 us
    gather x0 -> x1, local copies, waits for them, and re-layouts: none -> 10.4 us  [gather_around(): pieces = jnp.stack(pieces)[(index - jnp.arange(length)) % length]]
    all_gather x1, waiting for transfers between devices: 10.1 us -> 0.01 us  [on_device(): full_rows = lax.all_gather(normed, 'tp', axis=0, tiled=True)]
  transfers between devices with their start and end apart: 6 -> 20, of which waited for: 6 -> 17; matrix products, arithmetic and copies ran while one was open for 1% -> 6% of each run, Pallas kernels for 0% -> 0%
where the time goes in v1:
time: 959 us; the launch traced here: 945 us
  waiting for transfers between devices  479 us (50%)
  local copies, waits for them, and re-layouts  168 us (18%)
  blocking collectives  154 us (16%)
  matrix products  69.4 us (7%)
  other arithmetic  57.2 us (6%)
  between operations  14.3 us (1%)
    ppermute x15, waiting for transfers between devices, gather_around(): pieces.append(lax.ppermute(pieces[-1], axis, right))  463 us
    all_gather x4, blocking collectives, prefix(): pieces = jax.tree.map(lambda part: lax.all_gather(part, axis), value)  154 us
    dot_general x1, matrix products, on_device(): jnp.dot(hidden, down_columns, preferred_element_type=jnp.float32)  27.4 us
    dynamic_slice x30, local copies, waits for them, and re-layouts, step(): longer = join(subtotal, jax.tree.map(lambda part: part[position], pieces))  26.7 us
    mul x3, local copies, waits for them, and re-layouts, spread_blocks(): unit_blocks * turned  23.5 us
  transfers between devices with their start and end apart: 20, of which 17 were waited for; matrix products, arithmetic and copies ran while one was open for 6% of the time, Pallas kernels for 0%

profile of v1, /device:TPU:0, one launch (start us, length us, event | category | flops | bytes accessed | tf_op | source)
XLA Modules:
  0.0 945.3 jit_solution(1930564569433427898)
XLA Ops:
  9.7 8.3 broadcast_multiply_fusion.2
  18.1 7.8 mul.1865
  25.9 7.9 mul.1870
  33.8 10.5 %fusion.11 = f32[512,4096]{1,0:T(8,128)S(1)} fusion(bf16[512,512]{1,0:T(8,128)(2,1)S(1)} %copy-done.31, f32[512,2048]{1,0:T(8,128)} %mul.1870, f32[512,2048]{1,0:T(8,128)} %mul.1865), kind=kOutput, calls=%fused_computation.19 | convolution fusion | flops 12886999040 | bytes 17301504 | tf_op jit(solution)/shard_map/dot_general | solution.py:155
  45.4 2.5 fusion.63
  47.9 2.7 fusion.64
  50.6 3.0 bitcast_add_fusion.9
  53.7 5.1 multiply_subtract_fusion.3
  58.8 1.4 copy.145
  61.5 6.0 copy_add_fusion.1
  67.5 4.0 bitcast_add_fusion.1
  77.4 2.5 copy.137
  79.9 2.4 copy.140
  82.3 2.4 copy.141
  84.7 2.4 copy.142
  87.2 2.4 copy.143
  89.5 2.4 copy.144
  92.6 43.2 %all-gather.2 = f32[16,1,2048]{2,1,0:T(1,128)S(1)} all-gather(f32[1,1,2048]{2,1,0:T(1,128)S(1)} %slice_bitcast_fusion.3), channel_id=1, replica_groups=mesh['sp'=16,'tp'=2] {'sp'}, dimensions={0}, use_global_device_ids=true | all-gather | bytes 139264 | tf_op jit(solution)/shard_map/all_gather | solution.py:26
  136.6 36.2 %all-gather.1 = f32[16,1,2048]{2,1,0:T(1,128)S(1)} all-gather(f32[1,1,2048]{2,1,0:T(1,128)S(1)} %slice_bitcast_fusion.4), channel_id=1, replica_groups=mesh['sp'=16,'tp'=2] {'sp'}, dimensions={0}, use_global_device_ids=true | all-gather | bytes 139264 | tf_op jit(solution)/shard_map/all_gather | solution.py:26
  173.5 38.1 %all-gather = f32[16,1,2048]{2,1,0:T(1,128)S(1)} all-gather(f32[1,1,2048]{2,1,0:T(1,128)S(1)} %slice_bitcast_fusion.5), channel_id=1, replica_groups=mesh['sp'=16,'tp'=2] {'sp'}, dimensions={0}, use_global_device_ids=true | all-gather | bytes 139264 | tf_op jit(solution)/shard_map/all_gather | solution.py:26
  212.4 36.3 %all-gather.3 = f32[16,1,2048]{2,1,0:T(1,128)S(1)} all-gather(f32[1,1,2048]{2,1,0:T(1,128)S(1)} %slice_bitcast_fusion.2), channel_id=1, replica_groups=mesh['sp'=16,'tp'=2] {'sp'}, dimensions={0}, use_global_device_ids=true | all-gather | bytes 139264 | tf_op jit(solution)/shard_map/all_gather | solution.py:26
  249.3 27.6 %while.16 = (s32[]{:T(128)}, f32[2048]{0:T(1024)S(1)}, f32[2048]{0:T(1024)S(1)}, s32[]{:T(128)}, f32[16,2048]{1,0:T(8,128)}, /*index=5*/f32[16,2048]{1,0:T(8,128...) while((s32[]{:T(128)}, f32[2048]{0:T(1024)S(1)}, f32[2048]{0:T(1024)S(1)}, ...), condition=%wide.region_1.2_spmd.clone, body=%wide.region_0.1_spmd.clone.sunk | while | flops 24580 | bytes 131201 | solution.py:35
  277.0 2.0 concatenate.124
  278.9 1.9 concatenate.129
  280.8 1.9 concatenate.125
  282.7 2.4 copy.132
  285.1 2.4 copy.133
  287.5 2.4 copy.134
  289.9 1.3 copy.135
  291.2 1.3 copy.136
  292.8 8.1 broadcast_multiply_fusion
  300.9 7.8 mul.2031
  308.7 7.8 neg.11
  316.5 1.9 concatenate.128
  318.4 11.9 %stack.72 = f32[64,8,2048]{2,1,0:T(8,128)} concatenate(f32[64,1,2048]{2,1,0:T(1,128)S(1)} %get-tuple-element.246, f32[64,1,2048]{2,1,0:T(1,128)} %copy.140, f32[64,1,2048]{2,1,0:T(1,128)} %copy.141, f32[64,1,2048]{2,1,0:T(1,128)} %copy.142, f32[64,1,2048]{2,1,0:T(1,128)} %copy.143, f32[64,1,2048]{2,1,0:T(1,128)} %copy.144, f32[64,1,2048]{2,1,0:T(1,128)} %copy.145, ...), dimensions={1} | concatenate | bytes 8388608 | tf_op jit(solution)/shard_map/stack | solution.py:93
  330.4 12.0 %stack.71 = f32[64,8,2048]{2,1,0:T(8,128)} concatenate(f32[64,1,2048]{2,1,0:T(1,128)S(1)} %get-tuple-element.248, f32[64,1,2048]{2,1,0:T(1,128)} %copy.132, f32[64,1,2048]{2,1,0:T(1,128)} %copy.133, f32[64,1,2048]{2,1,0:T(1,128)} %copy.134, f32[64,1,2048]{2,1,0:T(1,128)} %copy.135, f32[64,1,2048]{2,1,0:T(1,128)} %copy.136, f32[64,1,2048]{2,1,0:T(1,128)} %copy.137, ...), dimensions={1} | concatenate | bytes 8388608 | tf_op jit(solution)/shard_map/stack | solution.py:92
  342.4 7.0 fusion.15
  350.3 16.5 %fusion.24 = bf16[512,512]{1,0:T(8,128)(2,1)S(1)} fusion(bf16[512,512]{1,0:T(8,128)(2,1)S(1)} %copy-done.32, f32[2048,512]{0,1:T(8,128)S(1)} %copy-done.19, f32[2048,512]{0,1:T(8,128)S(1)} %copy-done.18, f32[512,2048]{1,0:T(8,128)} %get-tuple-element.258, f32[512,2048]{1,0:T(8,128)S(1)} %get-tuple-element.257, f32[512]{0:T(512)S(1)} %copy-done.42), kind=kOutput, calls=%fused_computation.50 | convolution fusion | flops 12892241920 | bytes 17827840 | tf_op jit(solution)/shard_map/dot_general | solution.py:169
  366.8 2.6 convolution_convert_fusion.1
  369.5 7.5 reduce-scatter.3.cloned.1.call-done
  377.0 1.6 multiply_reduce_fusion
  378.6 2.6 multiply_convert_fusion.1
  382.6 1.9 collective-permute-start
  384.5 20.2 %collective-permute-done = bf16[2816,128]{1,0:T(8,128)(2,1)S(1)} collective-permute-done((bf16[2816,128]{1,0:T(8,128)(2,1)S(1)}, bf16[2816,128]{1,0:T(8,128)(2,1)S(1)}, u32[]{:S(2)}, u32[]{:S(2)}) %collective-permute-start) | collective-permute-done | bytes 720928 | tf_op jit(solution)/shard_map/ppermute | solution.py:18
  404.7 35.7 %collective-permute-done.1 = bf16[2816,128]{1,0:T(8,128)(2,1)S(1)} collective-permute-done((bf16[2816,128]{1,0:T(8,128)(2,1)S(1)}, bf16[2816,128]{1,0:T(8,128)(2,1)S(1)}, u32[]{:S(2)}, u32[]{:S(2)}) %collective-permute-start.1) | collective-permute-done | bytes 720928 | tf_op jit(solution)/shard_map/ppermute | solution.py:18
  440.4 34.3 %collective-permute-done.2 = bf16[2816,128]{1,0:T(8,128)(2,1)S(1)} collective-permute-done((bf16[2816,128]{1,0:T(8,128)(2,1)S(1)}, bf16[2816,128]{1,0:T(8,128)(2,1)S(1)}, u32[]{:S(2)}, u32[]{:S(2)}) %collective-permute-start.2) | collective-permute-done | bytes 720928 | tf_op jit(solution)/shard_map/ppermute | solution.py:18
  474.8 32.9 %collective-permute-done.3 = bf16[2816,128]{1,0:T(8,128)(2,1)S(1)} collective-permute-done((bf16[2816,128]{1,0:T(8,128)(2,1)S(1)}, bf16[2816,128]{1,0:T(8,128)(2,1)S(1)}, u32[]{:S(2)}, u32[]{:S(2)}) %collective-permute-start.3) | collective-permute-done | bytes 720928 | tf_op jit(solution)/shard_map/ppermute | solution.py:18
  507.7 37.2 %collective-permute-done.4 = bf16[2816,128]{1,0:T(8,128)(2,1)S(1)} collective-permute-done((bf16[2816,128]{1,0:T(8,128)(2,1)S(1)}, bf16[2816,128]{1,0:T(8,128)(2,1)S(1)}, u32[]{:S(2)}, u32[]{:S(2)}) %collective-permute-start.4) | collective-permute-done | bytes 720928 | tf_op jit(solution)/shard_map/ppermute | solution.py:18
  544.9 37.6 %collective-permute-done.5 = bf16[2816,128]{1,0:T(8,128)(2,1)S(1)} collective-permute-done((bf16[2816,128]{1,0:T(8,128)(2,1)S(1)}, bf16[2816,128]{1,0:T(8,128)(2,1)S(1)}, u32[]{:S(2)}, u32[]{:S(2)}) %collective-permute-start.5) | collective-permute-done | bytes 720928 | tf_op jit(solution)/shard_map/ppermute | solution.py:18
  582.5 38.0 %collective-permute-done.6 = bf16[2816,128]{1,0:T(8,128)(2,1)S(1)} collective-permute-done((bf16[2816,128]{1,0:T(8,128)(2,1)S(1)}, bf16[2816,128]{1,0:T(8,128)(2,1)S(1)}, u32[]{:S(2)}, u32[]{:S(2)}) %collective-permute-start.6) | collective-permute-done | bytes 720928 | tf_op jit(solution)/shard_map/ppermute | solution.py:18
  621.4 24.9 %collective-permute-done.7 = bf16[2816,128]{1,0:T(8,128)(2,1)S(1)} collective-permute-done((bf16[2816,128]{1,0:T(8,128)(2,1)S(1)}, bf16[2816,128]{1,0:T(8,128)(2,1)S(1)}, u32[]{:S(2)}, u32[]{:S(2)}) %collective-permute-start.7) | collective-permute-done | bytes 720928 | tf_op jit(solution)/shard_map/ppermute | solution.py:18
  648.2 25.1 %collective-permute-done.8 = bf16[2816,128]{1,0:T(8,128)(2,1)S(1)} collective-permute-done((bf16[2816,128]{1,0:T(8,128)(2,1)S(1)}, bf16[2816,128]{1,0:T(8,128)(2,1)S(1)}, u32[]{:S(2)}, u32[]{:S(2)}) %collective-permute-start.8) | collective-permute-done | bytes 720928 | tf_op jit(solution)/shard_map/ppermute | solution.py:18
  675.1 34.1 %collective-permute-done.9 = bf16[2816,128]{1,0:T(8,128)(2,1)S(1)} collective-permute-done((bf16[2816,128]{1,0:T(8,128)(2,1)S(1)}, bf16[2816,128]{1,0:T(8,128)(2,1)S(1)}, u32[]{:S(2)}, u32[]{:S(2)}) %collective-permute-start.9) | collective-permute-done | bytes 720928 | tf_op jit(solution)/shard_map/ppermute | solution.py:18
  710.9 26.1 %collective-permute-done.10 = bf16[2816,128]{1,0:T(8,128)(2,1)S(1)} collective-permute-done((bf16[2816,128]{1,0:T(8,128)(2,1)S(1)}, bf16[2816,128]{1,0:T(8,128)(2,1)S(1)}, u32[]{:S(2)}, u32[]{:S(2)}) %collective-permute-start.10) | collective-permute-done | bytes 720928 | tf_op jit(solution)/shard_map/ppermute | solution.py:18
  738.9 35.6 %collective-permute-done.11 = bf16[2816,128]{1,0:T(8,128)(2,1)S(1)} collective-permute-done((bf16[2816,128]{1,0:T(8,128)(2,1)S(1)}, bf16[2816,128]{1,0:T(8,128)(2,1)S(1)}, u32[]{:S(2)}, u32[]{:S(2)}) %collective-permute-start.11) | collective-permute-done | bytes 720928 | tf_op jit(solution)/shard_map/ppermute | solution.py:18
  776.3 33.2 %collective-permute-done.12 = bf16[2816,128]{1,0:T(8,128)(2,1)S(1)} collective-permute-done((bf16[2816,128]{1,0:T(8,128)(2,1)S(1)}, bf16[2816,128]{1,0:T(8,128)(2,1)S(1)}, u32[]{:S(2)}, u32[]{:S(2)}) %collective-permute-start.12) | collective-permute-done | bytes 720928 | tf_op jit(solution)/shard_map/ppermute | solution.py:18
  811.4 35.4 %collective-permute-done.13 = bf16[2816,128]{1,0:T(8,128)(2,1)S(1)} collective-permute-done((bf16[2816,128]{1,0:T(8,128)(2,1)S(1)}, bf16[2816,128]{1,0:T(8,128)(2,1)S(1)}, u32[]{:S(2)}, u32[]{:S(2)}) %collective-permute-start.13) | collective-permute-done | bytes 720928 | tf_op jit(solution)/shard_map/ppermute | solution.py:18
  848.9 13.0 %collective-permute-done.14 = bf16[2816,128]{1,0:T(8,128)(2,1)S(1)} collective-permute-done((bf16[2816,128]{1,0:T(8,128)(2,1)S(1)}, bf16[2816,128]{1,0:T(8,128)(2,1)S(1)}, u32[]{:S(2)}, u32[]{:S(2)}) %collective-permute-start.14) | collective-permute-done | bytes 720928 | tf_op jit(solution)/shard_map/ppermute | solution.py:18
  862.8 10.4 %gather_fusion = bf16[16,2816,128]{2,1,0:T(8,128)(2,1)} fusion(bf16[16,2816,128]{2,1,0:T(8,128)(2,1)} %bitcast_dynamic-update-slice_fusion, s32[1024]{0:T(1024)S(1)} %pad_clamp_fusion), kind=kCustom, calls=%fused_computation | custom fusion | bytes 23068736 | tf_op jit(solution)/shard_map/gather | solution.py:20
  873.2 14.9 %copy.148 = bf16[2816,16,128]{0,2,1:T(8,128)(2,1)} copy(bf16[2816,16,128]{2,0,1:T(8,128)(2,1)} %bitcast.240) | data formatting | bytes 23068672 | tf_op jit(solution)/shard_map/transpose | solution.py:10
  888.2 12.5 %fusion.65 = f32[512,2816]{1,0:T(8,128)} fusion(bf16[512,2048]{1,0:T(8,128)(2,1)} %all-gather.8.cloned.1.call-done, bf16[2048,2816]{1,0:T(8,128)(2,1)} %all-gather.10.cloned.1.call-done), kind=kOutput, calls=%fused_computation.207 | convolution fusion | flops 5905580032 | bytes 19398656 | tf_op jit(solution)/shard_map/dot_general | solution.py:189
  900.6 27.4 %convolution_convert_fusion = bf16[512,2048]{1,0:T(8,128)(2,1)} fusion(bf16[2816,2048]{0,1:T(8,128)(2,1)} %bitcast.241, f32[512,2816]{1,0:T(8,128)} %fusion.65, bf16[512,2048]{1,0:T(8,128)(2,1)} %all-gather.8.cloned.1.call-done, bf16[2048,2816]{1,0:T(8,128)(2,1)} %all-gather.12.cloned.1.call-done), kind=kOutput, calls=%fused_computation.36 | convolution fusion | flops 11820859392 | bytes 33030144 | tf_op jit(solution)/shard_map/dot_general | solution.py:201
  928.0 7.3 reduce-scatter.5.cloned.1.call-done
  935.3 3.1 add_convert_fusion
  (231 shorter events, 59.2 us)
Async XLA Ops:
  6.5 360.3 %copy-start = (bf16[512,2048]{1,0:T(8,128)(2,1)S(1)}, bf16[512,2048]{1,0:T(8,128)(2,1)}, u32[]{:S(2)}) copy-start(bf16[512,2048]{1,0:T(8,128)(2,1)} %param.27) | copy-start | bytes 6291460
  6.5 370.4 %reduce-scatter.3.cloned.1.call-start = ((), (), s32[]{:S(2)}) async-start(), calls=%async_computation.2 | async-start | bytes 3145728 | tf_op jit(solution)/shard_map/reduce_scatter | solution.py:179
  6.5 11.5 %copy-start.39 = (f32[32,32]{0,1:T(8,128)}, f32[32,32]{0,1:T(8,128)S(1)}, u32[]{:S(2)}) copy-start(f32[32,32]{0,1:T(8,128)S(1)} %fusion.52) | copy-start | bytes 12292
  25.9 7.9 copy-start.31
  45.3 5.2 copy-start.2
  45.3 5.2 copy-start.3
  47.8 5.8 copy-start.5
  47.9 5.8 copy-start.13
  47.9 5.8 copy-start.14
  50.6 8.2 copy-start.7
  50.6 8.2 copy-start.15
  50.6 8.2 copy-start.16
  58.8 1.4 copy-start.17
  61.3 10.9 %copy-start.33 = (f32[8,2048]{1,0:T(8,128)}, f32[8,2048]{1,0:T(8,128)S(1)}, u32[]{:S(2)}) copy-start(f32[8,2048]{1,0:T(8,128)S(1)} %concatenate.100) | copy-start | bytes 196612
  61.4 10.8 %copy-start.35 = (f32[8,2048]{1,0:T(8,128)}, f32[8,2048]{1,0:T(8,128)S(1)}, u32[]{:S(2)}) copy-start(f32[8,2048]{1,0:T(8,128)S(1)} %concatenate.102) | copy-start | bytes 196612
  61.4 10.0 %copy-start.6 = (f32[64,1,2048]{2,1,0:T(1,128)S(1)}, f32[64,1,2048]{2,1,0:T(1,128)}, u32[]{:S(2)}) copy-start(f32[64,1,2048]{2,1,0:T(1,128)} %copy-done.5) | copy-start | bytes 1572868
  61.4 10.0 %copy-start.8 = (f32[64,1,2048]{2,1,0:T(1,128)S(1)}, f32[64,1,2048]{2,1,0:T(1,128)}, u32[]{:S(2)}) copy-start(f32[64,1,2048]{2,1,0:T(1,128)} %copy-done.7) | copy-start | bytes 1572868
  75.5 1.1 copy-start.9
  75.5 1.9 copy-start.11
  77.3 14.6 %copy-start.21 = (f32[64,2048]{1,0:T(8,128)S(1)}, f32[64,2048]{1,0:T(8,128)}, u32[]{:S(2)}) copy-start(f32[64,2048]{1,0:T(8,128)} %fusion.38) | copy-start | bytes 1572868
  77.4 14.6 %copy-start.20 = (f32[64,2048]{1,0:T(8,128)S(1)}, f32[64,2048]{1,0:T(8,128)}, u32[]{:S(2)}) copy-start(f32[64,2048]{1,0:T(8,128)} %get-tuple-element.206) | copy-start | bytes 1572868
  77.4 14.6 %copy-start.10 = (f32[64,2048]{1,0:T(8,128)S(1)}, f32[64,2048]{1,0:T(8,128)}, u32[]{:S(2)}) copy-start(f32[64,2048]{1,0:T(8,128)} %copy-done.9) | copy-start | bytes 1572868
  77.4 14.6 %copy-start.12 = (f32[64,2048]{1,0:T(8,128)S(1)}, f32[64,2048]{1,0:T(8,128)}, u32[]{:S(2)}) copy-start(f32[64,2048]{1,0:T(8,128)} %copy-done.11) | copy-start | bytes 1572868
  77.4 14.6 %copy-start.29 = (f32[48,2048]{1,0:T(8,128)S(1)}, f32[48,2048]{1,0:T(8,128)}, u32[]{:S(2)}) copy-start(f32[48,2048]{1,0:T(8,128)} %slice.236) | copy-start | bytes 1179652
  92.3 120.1 %copy-start.22 = (f32[64,2048]{1,0:T(8,128)}, f32[64,2048]{1,0:T(8,128)S(1)}, u32[]{:S(2)}) copy-start(f32[64,2048]{1,0:T(8,128)S(1)} %get-tuple-element.203) | copy-start | bytes 1572868
  92.6 119.8 %copy-start.23 = (f32[64,2048]{1,0:T(8,128)}, f32[64,2048]{1,0:T(8,128)S(1)}, u32[]{:S(2)}) copy-start(f32[64,2048]{1,0:T(8,128)S(1)} %get-tuple-element.262) | copy-start | bytes 1572868
  92.6 156.1 %copy-start.24 = (f32[64,2048]{1,0:T(8,128)}, f32[64,2048]{1,0:T(8,128)S(1)}, u32[]{:S(2)}) copy-start(f32[64,2048]{1,0:T(8,128)S(1)} %get-tuple-element.261) | copy-start | bytes 1572868
  92.6 156.1 %copy-start.25 = (f32[64,2048]{1,0:T(8,128)}, f32[64,2048]{1,0:T(8,128)S(1)}, u32[]{:S(2)}) copy-start(f32[64,2048]{1,0:T(8,128)S(1)} %get-tuple-element.267) | copy-start | bytes 1572868
  92.6 200.0 %copy-start.37 = (f32[32,16,64]{2,1,0:T(8,128)S(1)}, f32[32,16,64]{2,1,0:T(8,128)}, u32[]{:S(2)}) copy-start(f32[32,16,64]{2,1,0:T(8,128)} %param.24) | copy-start | bytes 393220
  172.8 120.0 %copy-start.40 = (f32[32,32]{0,1:T(8,128)S(1)}, f32[32,32]{0,1:T(8,128)}, u32[]{:S(2)}) copy-start(f32[32,32]{0,1:T(8,128)} %copy-done.39) | copy-start | bytes 12292
  276.9 13.0 %copy-start.27 = (f32[64,1,2048]{2,0,1:T(8,128)S(1)}, f32[64,1,2048]{2,0,1:T(8,128)}, u32[]{:S(2)}) copy-start(f32[64,1,2048]{2,0,1:T(8,128)} %get-tuple-element.195) | copy-start | bytes 1572868
  276.9 14.3 %copy-start.26 = (f32[64,1,2048]{2,0,1:T(8,128)S(1)}, f32[64,1,2048]{2,0,1:T(8,128)}, u32[]{:S(2)}) copy-start(f32[64,1,2048]{2,0,1:T(8,128)} %get-tuple-element.193) | copy-start | bytes 1572868
  276.9 15.7 %copy-start.38 = (f32[32,16,64]{2,1,0:T(8,128)S(1)}, f32[32,16,64]{2,1,0:T(8,128)}, u32[]{:S(2)}) copy-start(f32[32,16,64]{2,1,0:T(8,128)} %param.25) | copy-start | bytes 393220
  330.3 12.0 %copy-start.28 = (f32[64,2048]{1,0:T(8,128)S(1)}, f32[64,2048]{1,0:T(8,128)}, u32[]{:S(2)}) copy-start(f32[64,2048]{1,0:T(8,128)} %concatenate.124) | copy-start | bytes 1572868
  330.3 12.0 %copy-start.34 = (f32[8,2048]{1,0:T(8,128)S(1)}, f32[8,2048]{1,0:T(8,128)}, u32[]{:S(2)}) copy-start(f32[8,2048]{1,0:T(8,128)} %copy-done.33) | copy-start | bytes 196612
  330.3 12.0 %copy-start.36 = (f32[8,2048]{1,0:T(8,128)S(1)}, f32[8,2048]{1,0:T(8,128)}, u32[]{:S(2)}) copy-start(f32[8,2048]{1,0:T(8,128)} %copy-done.35) | copy-start | bytes 196612
  342.3 7.0 copy-start.18
  342.4 7.9 copy-start.19
  342.4 7.9 copy-start.32
  342.4 7.9 copy-start.42
  366.8 10.2 %copy-start.4 = (bf16[256,2048]{1,0:T(8,128)(2,1)S(1)}, bf16[256,2048]{1,0:T(8,128)(2,1)}, u32[]{:S(2)}) copy-start(bf16[256,2048]{1,0:T(8,128)(2,1)} %param.18) | copy-start | bytes 3145732
  366.8 11.8 %copy-start.41 = (f32[2048]{0:T(1024)S(1)}, f32[2048]{0:T(1024)}, u32[]{:S(2)}) copy-start(f32[2048]{0:T(1024)} %param.28) | copy-start | bytes 24580
  369.4 13.2 %copy-start.30 = (bf16[2816,128]{1,0:T(8,128)(2,1)S(1)}, bf16[2816,128]{1,0:T(8,128)(2,1)}, u32[]{:S(2)}) copy-start(bf16[2816,128]{1,0:T(8,128)(2,1)} %param.31) | copy-start | bytes 2162692
  369.4 518.7 %all-gather.8.cloned.1.call-start = ((), (), s32[]{:S(2)}) async-start(), calls=%async_computation.3 | async-start | bytes 3145728 | tf_op jit(solution)/shard_map/all_gather | solution.py:188
  381.3 506.9 %all-gather.10.cloned.1.call-start = ((), (), s32[]{:S(2)}) async-start(), calls=%async_computation.4 | async-start | bytes 12255232 | tf_op jit(solution)/shard_map/all_gather | solution.py:191
  382.0 518.6 %all-gather.12.cloned.1.call-start = ((), (), s32[]{:S(2)}) async-start(), calls=%async_computation.5 | async-start | bytes 12255232 | tf_op jit(solution)/shard_map/all_gather | solution.py:196
  382.6 552.7 %reduce-scatter.5.cloned.1.call-start = ((), (), s32[]{:S(2)}) async-start(), calls=%async_computation.6 | async-start | bytes 3145728 | tf_op jit(solution)/shard_map/reduce_scatter | solution.py:204
  382.6 22.1 %collective-permute-start = (bf16[2816,128]{1,0:T(8,128)(2,1)S(1)}, bf16[2816,128]{1,0:T(8,128)(2,1)S(1)}, u32[]{:S(2)}, u32[]{:S(2)}) collective-permute-start(bf16[2816,128]{1,0:T(8,128)(2,1)S(1)} %copy-done.30), channel_id=1, source_target_pairs={{0,2},{2,4},{4,6},{6,8},{8,10},{10,12},{12,14},{14,16},{16,18},{18... | collective-permute-start | bytes 2162696 | tf_op jit(solution)/shard_map/ppermute | solution.py:18
  404.7 35.7 %collective-permute-start.1 = (bf16[2816,128]{1,0:T(8,128)(2,1)S(1)}, bf16[2816,128]{1,0:T(8,128)(2,1)S(1)}, u32[]{:S(2)}, u32[]{:S(2)}) collective-permute-start(bf16[2816,128]{1,0:T(8,128)(2,1)S(1)} %collective-permute-done), channel_id=1, source_target_pairs={{0,2},{2,4},{4,6},{6,8},{8,10},{10,12},{12,14},{14,16},{16,18},{18... | collective-permute-start | bytes 2162696 | tf_op jit(solution)/shard_map/ppermute | solution.py:18
  440.4 34.3 %collective-permute-start.2 = (bf16[2816,128]{1,0:T(8,128)(2,1)S(1)}, bf16[2816,128]{1,0:T(8,128)(2,1)S(1)}, u32[]{:S(2)}, u32[]{:S(2)}) collective-permute-start(bf16[2816,128]{1,0:T(8,128)(2,1)S(1)} %collective-permute-done.1), channel_id=1, source_target_pairs={{0,2},{2,4},{4,6},{6,8},{8,10},{10,12},{12,14},{14,16},{16,18},{18... | collective-permute-start | bytes 2162696 | tf_op jit(solution)/shard_map/ppermute | solution.py:18
  474.8 32.9 %collective-permute-start.3 = (bf16[2816,128]{1,0:T(8,128)(2,1)S(1)}, bf16[2816,128]{1,0:T(8,128)(2,1)S(1)}, u32[]{:S(2)}, u32[]{:S(2)}) collective-permute-start(bf16[2816,128]{1,0:T(8,128)(2,1)S(1)} %collective-permute-done.2), channel_id=1, source_target_pairs={{0,2},{2,4},{4,6},{6,8},{8,10},{10,12},{12,14},{14,16},{16,18},{18... | collective-permute-start | bytes 2162696 | tf_op jit(solution)/shard_map/ppermute | solution.py:18
  507.7 37.2 %collective-permute-start.4 = (bf16[2816,128]{1,0:T(8,128)(2,1)S(1)}, bf16[2816,128]{1,0:T(8,128)(2,1)S(1)}, u32[]{:S(2)}, u32[]{:S(2)}) collective-permute-start(bf16[2816,128]{1,0:T(8,128)(2,1)S(1)} %collective-permute-done.3), channel_id=1, source_target_pairs={{0,2},{2,4},{4,6},{6,8},{8,10},{10,12},{12,14},{14,16},{16,18},{18... | collective-permute-start | bytes 2162696 | tf_op jit(solution)/shard_map/ppermute | solution.py:18
  544.9 37.6 %collective-permute-start.5 = (bf16[2816,128]{1,0:T(8,128)(2,1)S(1)}, bf16[2816,128]{1,0:T(8,128)(2,1)S(1)}, u32[]{:S(2)}, u32[]{:S(2)}) collective-permute-start(bf16[2816,128]{1,0:T(8,128)(2,1)S(1)} %collective-permute-done.4), channel_id=1, source_target_pairs={{0,2},{2,4},{4,6},{6,8},{8,10},{10,12},{12,14},{14,16},{16,18},{18... | collective-permute-start | bytes 2162696 | tf_op jit(solution)/shard_map/ppermute | solution.py:18
  582.5 38.0 %collective-permute-start.6 = (bf16[2816,128]{1,0:T(8,128)(2,1)S(1)}, bf16[2816,128]{1,0:T(8,128)(2,1)S(1)}, u32[]{:S(2)}, u32[]{:S(2)}) collective-permute-start(bf16[2816,128]{1,0:T(8,128)(2,1)S(1)} %collective-permute-done.5), channel_id=1, source_target_pairs={{0,2},{2,4},{4,6},{6,8},{8,10},{10,12},{12,14},{14,16},{16,18},{18... | collective-permute-start | bytes 2162696 | tf_op jit(solution)/shard_map/ppermute | solution.py:18
  620.5 25.9 %collective-permute-start.7 = (bf16[2816,128]{1,0:T(8,128)(2,1)S(1)}, bf16[2816,128]{1,0:T(8,128)(2,1)S(1)}, u32[]{:S(2)}, u32[]{:S(2)}) collective-permute-start(bf16[2816,128]{1,0:T(8,128)(2,1)S(1)} %collective-permute-done.6), channel_id=1, source_target_pairs={{0,2},{2,4},{4,6},{6,8},{8,10},{10,12},{12,14},{14,16},{16,18},{18... | collective-permute-start | bytes 2162696 | tf_op jit(solution)/shard_map/ppermute | solution.py:18
  646.3 26.9 %collective-permute-start.8 = (bf16[2816,128]{1,0:T(8,128)(2,1)S(1)}, bf16[2816,128]{1,0:T(8,128)(2,1)S(1)}, u32[]{:S(2)}, u32[]{:S(2)}) collective-permute-start(bf16[2816,128]{1,0:T(8,128)(2,1)S(1)} %collective-permute-done.7), channel_id=1, source_target_pairs={{0,2},{2,4},{4,6},{6,8},{8,10},{10,12},{12,14},{14,16},{16,18},{18... | collective-permute-start | bytes 2162696 | tf_op jit(solution)/shard_map/ppermute | solution.py:18
  673.3 35.9 %collective-permute-start.9 = (bf16[2816,128]{1,0:T(8,128)(2,1)S(1)}, bf16[2816,128]{1,0:T(8,128)(2,1)S(1)}, u32[]{:S(2)}, u32[]{:S(2)}) collective-permute-start(bf16[2816,128]{1,0:T(8,128)(2,1)S(1)} %collective-permute-done.8), channel_id=1, source_target_pairs={{0,2},{2,4},{4,6},{6,8},{8,10},{10,12},{12,14},{14,16},{16,18},{18... | collective-permute-start | bytes 2162696 | tf_op jit(solution)/shard_map/ppermute | solution.py:18
  709.1 27.9 %collective-permute-start.10 = (bf16[2816,128]{1,0:T(8,128)(2,1)S(1)}, bf16[2816,128]{1,0:T(8,128)(2,1)S(1)}, u32[]{:S(2)}, u32[]{:S(2)}) collective-permute-start(bf16[2816,128]{1,0:T(8,128)(2,1)S(1)} %collective-permute-done.9), channel_id=1, source_target_pairs={{0,2},{2,4},{4,6},{6,8},{8,10},{10,12},{12,14},{14,16},{16,18},{18... | collective-permute-start | bytes 2162696 | tf_op jit(solution)/shard_map/ppermute | solution.py:18
  737.1 37.5 %collective-permute-start.11 = (bf16[2816,128]{1,0:T(8,128)(2,1)S(1)}, bf16[2816,128]{1,0:T(8,128)(2,1)S(1)}, u32[]{:S(2)}, u32[]{:S(2)}) collective-permute-start(bf16[2816,128]{1,0:T(8,128)(2,1)S(1)} %collective-permute-done.10), channel_id=1, source_target_pairs={{0,2},{2,4},{4,6},{6,8},{8,10},{10,12},{12,14},{14,16},{16,18},{18... | collective-permute-start | bytes 2162696 | tf_op jit(solution)/shard_map/ppermute | solution.py:18
  774.5 35.0 %collective-permute-start.12 = (bf16[2816,128]{1,0:T(8,128)(2,1)S(1)}, bf16[2816,128]{1,0:T(8,128)(2,1)S(1)}, u32[]{:S(2)}, u32[]{:S(2)}) collective-permute-start(bf16[2816,128]{1,0:T(8,128)(2,1)S(1)} %collective-permute-done.11), channel_id=1, source_target_pairs={{0,2},{2,4},{4,6},{6,8},{8,10},{10,12},{12,14},{14,16},{16,18},{18... | collective-permute-start | bytes 2162696 | tf_op jit(solution)/shard_map/ppermute | solution.py:18
  809.6 37.2 %collective-permute-start.13 = (bf16[2816,128]{1,0:T(8,128)(2,1)S(1)}, bf16[2816,128]{1,0:T(8,128)(2,1)S(1)}, u32[]{:S(2)}, u32[]{:S(2)}) collective-permute-start(bf16[2816,128]{1,0:T(8,128)(2,1)S(1)} %collective-permute-done.12), channel_id=1, source_target_pairs={{0,2},{2,4},{4,6},{6,8},{8,10},{10,12},{12,14},{14,16},{16,18},{18... | collective-permute-start | bytes 2162696 | tf_op jit(solution)/shard_map/ppermute | solution.py:18
  846.8 15.1 %collective-permute-start.14 = (bf16[2816,128]{1,0:T(8,128)(2,1)S(1)}, bf16[2816,128]{1,0:T(8,128)(2,1)S(1)}, u32[]{:S(2)}, u32[]{:S(2)}) collective-permute-start(bf16[2816,128]{1,0:T(8,128)(2,1)S(1)} %collective-permute-done.13), channel_id=1, source_target_pairs={{0,2},{2,4},{4,6},{6,8},{8,10},{10,12},{12,14},{14,16},{16,18},{18... | collective-permute-start | bytes 2162696 | tf_op jit(solution)/shard_map/ppermute | solution.py:18
  900.6 37.7 %copy-start.1 = (bf16[512,2048]{1,0:T(8,128)(2,1)S(1)}, bf16[512,2048]{1,0:T(8,128)(2,1)}, u32[]{:S(2)}) copy-start(bf16[512,2048]{1,0:T(8,128)(2,1)} %param.27) | copy-start | bytes 6291460
Sparse Core Ops, SparseCore 0:
  369.6 7.3 reduce-scatter.2
  381.4 11.8 all-gather.7
  396.0 209.5 all-gather.9
  608.2 221.3 all-gather.11
  928.2 7.0 reduce-scatter.4
